TPU v7x, 32 devices: a whole 2x2x4 slice. The times are simulated.
32 devices in a mesh: grp: 2 (over y), sp: 4 (over z), tp: 4 (over x, core).
Axes of the slice: x: 2, y: 2, z: 4, core: 2. Of those that a mesh axis runs over, the one named last changes fastest.
Arguments:
- latent: bfloat16 [3072, 2048], P(('grp', 'sp')), parts along dimension 0, may hold values from -6 to 6
- conditioning: bfloat16 [4096], P(('grp', 'sp')), parts along dimension 0, may hold values from -6 to 6
- context: bfloat16 [128, 2048], P(('grp', 'sp')), parts along dimension 0, may hold values from -6 to 6
- ctx_vector: bfloat16 [2048], P('sp'), may hold values from -6 to 6
- w_shift: bfloat16 [2048, 2048], P('sp', 'tp'), may hold values from -0.25 to 0.25
- w_scale: bfloat16 [2048, 2048], P('sp', 'tp'), may hold values from -0.25 to 0.25
- w_gate: bfloat16 [2048, 2048], P('sp', 'tp'), may hold values from -0.25 to 0.25
- norm_gain: bfloat16 [2048], replicated, may hold values from 0.099609375 to 1.8984375
- w_query: bfloat16 [2048, 1024], P(None, 'tp'), may hold values from -1 to 1
- w_key: bfloat16 [2048, 1024], P(None, 'tp'), may hold values from -1 to 1
- w_value: bfloat16 [2048, 1024], P(None, 'tp'), may hold values from -0.125 to 0.125
- offset_bias: float32 [16, 15, 31], P('tp'), may hold values from 1.5 to 4.5
- w_out: bfloat16 [1024, 2048], P(None, 'tp'), may hold values from -0.75 to 0.75
Outputs:
- mixed_out: bfloat16 [3072, 2048], P(('grp', 'sp'), 'tp'), parts along dimension 0
There are 2 independent parts, one for each index of `grp`. A program takes and returns all parts, laid end to end along the dimension named above; an argument that names none is the same for every part. Nothing has to cross between parts.
All inputs are finite; a program needn't handle non-finite values.
Results may differ from a plain program's by a relative error of at most 0.011.
Values may be sent and summed in bfloat16 or wider, within the bound.
A program may use at most 64 MiB of HBM per device.

v0:
```python
import jax
import jax.numpy as jnp
from jax import lax
from jax.sharding import PartitionSpec as P

HEAD_DIM = 64
GRID_W = 64
WIN_H = 8
WIN_W = 16


EPSILON = 1e-06


def extended(block, sides, width):
    for axis, dim in sides:
        count = lax.axis_size(axis)
        forward = [(i, i + 1) for i in range(count - 1)]
        backward = [(target, source) for source, target in forward]
        low = lax.ppermute(
            lax.slice_in_dim(block, block.shape[dim] - width, None, axis=dim), axis, forward
        )
        high = lax.ppermute(lax.slice_in_dim(block, 0, width, axis=dim), axis, backward)
        block = jnp.concatenate([low, block, high], axis=dim)
    return block


def modulated_norm(inputs, norm_gain, shift_vec, scale_vec):
    floats = inputs.astype(jnp.float32)
    inverse = lax.rsqrt(jnp.mean(floats * floats, axis=-1, keepdims=True) + EPSILON)
    return (
        floats * inverse * norm_gain.astype(jnp.float32) * (1.0 + scale_vec) + shift_vec
    ).astype(jnp.bfloat16)


def project(inputs, weight):
    return jnp.dot(inputs, weight, preferred_element_type=jnp.float32).astype(jnp.bfloat16)


def local(
    latent,
    conditioning,
    context,
    ctx_vector,
    w_shift,
    w_scale,
    w_gate,
    norm_gain,
    w_query,
    w_key,
    w_value,
    offset_bias,
    w_out,
):
    cols_tp = w_shift.shape[1]
    tp_index = lax.axis_index("tp")
    cond_act = jax.nn.silu(conditioning.astype(jnp.float32)).astype(jnp.bfloat16)
    ctx_act = jax.nn.silu(ctx_vector.astype(jnp.float32)).astype(jnp.bfloat16)
    both_acts = jnp.stack([cond_act, ctx_act])
    part_shift = jnp.dot(both_acts, w_shift, preferred_element_type=jnp.float32)
    part_scale = jnp.dot(both_acts, w_scale, preferred_element_type=jnp.float32)
    part_gate = jnp.dot(cond_act, w_gate, preferred_element_type=jnp.float32)
    shift_own, scale_own, gate_vec = lax.psum((part_shift, part_scale, part_gate), "sp")
    shift_all, scale_all = (
        lax.all_gather(shift_own, "tp", axis=1, tiled=True),
        lax.all_gather(scale_own, "tp", axis=1, tiled=True),
    )
    normed = modulated_norm(latent, norm_gain, shift_all[0], scale_all[0])
    queries = project(normed, w_query)
    keys_lat = project(normed, w_key)
    values_lat = project(normed, w_value)
    head_width = w_query.shape[1]
    local_heads = head_width // HEAD_DIM
    ctx_normed = modulated_norm(context, norm_gain, shift_all[1], scale_all[1])
    ctx_pairs = lax.all_gather(
        jnp.concatenate([project(ctx_normed, w_key), project(ctx_normed, w_value)], axis=1),
        "sp",
        axis=0,
        tiled=True,
    )
    ctx_keys = ctx_pairs[:, :head_width].reshape(-1, local_heads, HEAD_DIM)
    ctx_values = ctx_pairs[:, head_width:].reshape(-1, local_heads, HEAD_DIM)
    rows_dev = latent.shape[0] // GRID_W
    key_value = jnp.concatenate([keys_lat, values_lat], axis=1).reshape(
        rows_dev, GRID_W, 2 * head_width
    )
    padded = extended(key_value, (("sp", 0),), WIN_H // 2)
    grid_rows = rows_dev * lax.axis_size("sp")
    row_base = lax.axis_index("sp") * rows_dev
    global_rows = row_base + jnp.arange(rows_dev, dtype=jnp.int32)
    first_rows = jnp.clip(global_rows - WIN_H // 2, 0, grid_rows - WIN_H)
    starts = first_rows - row_base + WIN_H // 2
    windows = jax.vmap(
        lambda window_start: lax.dynamic_slice_in_dim(padded, window_start, WIN_H, 0)
    )(starts)
    key_window = windows[..., :head_width].reshape(rows_dev, WIN_H, GRID_W, local_heads, HEAD_DIM)
    value_window = windows[..., head_width:].reshape(rows_dev, WIN_H, GRID_W, local_heads, HEAD_DIM)
    query_grid = queries.reshape(rows_dev, GRID_W, local_heads, HEAD_DIM)
    scale_qk = HEAD_DIM ** (-0.5)
    columns = jnp.arange(GRID_W, dtype=jnp.int32)
    col_first = jnp.clip(columns - WIN_W // 2, 0, GRID_W - WIN_W)
    inside = (columns[None, :] >= col_first[:, None]) & (
        columns[None, :] < col_first[:, None] + WIN_W
    )
    col_offset = jnp.clip(columns[None, :] - columns[:, None] + WIN_W - 1, 0, 2 * WIN_W - 2)
    table_cols = offset_bias[:, :, col_offset]
    row_offsets = first_rows - global_rows + WIN_H - 1
    table_rows = jax.vmap(
        lambda offset_row: lax.dynamic_slice_in_dim(table_cols, offset_row, WIN_H, 1)
    )(row_offsets)
    win_scores = (
        jnp.einsum("rchd,rijhd->rhcij", query_grid, key_window, preferred_element_type=jnp.float32)
        * scale_qk
    )
    win_scores = jnp.where(
        inside[None, None, :, None, :], win_scores + table_rows.transpose(0, 1, 3, 2, 4), -jnp.inf
    )
    ctx_scores = (
        jnp.einsum("rchd,lhd->rhcl", query_grid, ctx_keys, preferred_element_type=jnp.float32)
        * scale_qk
    )
    highest = jnp.maximum(jnp.max(win_scores, axis=(3, 4)), jnp.max(ctx_scores, axis=3))
    win_exp = jnp.exp(win_scores - highest[..., None, None])
    ctx_exp = jnp.exp(ctx_scores - highest[..., None])
    totals = jnp.sum(win_exp, axis=(3, 4)) + jnp.sum(ctx_exp, axis=3)
    win_weights = (win_exp / totals[..., None, None]).astype(jnp.bfloat16)
    ctx_weights = (ctx_exp / totals[..., None]).astype(jnp.bfloat16)
    attended = jnp.einsum(
        "rhcij,rijhd->rchd", win_weights, value_window, preferred_element_type=jnp.float32
    )
    attended = attended + jnp.einsum(
        "rhcl,lhd->rchd", ctx_weights, ctx_values, preferred_element_type=jnp.float32
    )
    attended = attended.astype(jnp.bfloat16).reshape(rows_dev * GRID_W, head_width)
    branch = jnp.dot(
        lax.all_gather(attended, "tp", axis=1, tiled=True),
        w_out,
        preferred_element_type=jnp.float32,
    )
    residual = lax.dynamic_slice_in_dim(latent, tp_index * cols_tp, cols_tp, 1).astype(jnp.float32)
    return (residual + gate_vec * branch).astype(jnp.bfloat16)


def solution(mesh):
    return jax.shard_map(
        local,
        mesh=mesh,
        in_specs=(
            P(("grp", "sp"), None),
            P(("grp", "sp")),
            P(("grp", "sp"), None),
            P("sp"),
            P("sp", "tp"),
            P("sp", "tp"),
            P("sp", "tp"),
            P(),
            P(None, "tp"),
            P(None, "tp"),
            P(None, "tp"),
            P("tp", None, None),
            P(None, "tp"),
        ),
        out_specs=P(("grp", "sp"), "tp"),
        check_vma=False,
    )
```

profile of v0, /device:TPU:0, one launch (start us, length us, event | category | flops | bytes accessed | tf_op | source)
XLA Modules:
  0.0 168.9 jit_solution(14793276694902223409)
XLA Ops:
  5.2 21.0 %all-reduce.1 = (f32[2,512]{1,0:T(2,128)S(1)}, f32[2,512]{1,0:T(2,128)S(1)}, f32[512]{0:T(512)}) all-reduce(f32[2,512]{1,0:T(2,128)S(1)} %fusion.39, f32[2,512]{1,0:T(2,128)S(1)} %fusion.40, f32[512]{0:T(512)S(1)} %bitcast.78), channel_id=1, replica_groups=mesh['grp'=2,'sp'=4,'tp'=4] {'sp'}, use_global_device_ids=true, to_apply=%region_3.4 | all-reduce | flops 2560 | bytes 20480 | tf_op jit(solution)/shard_map/psum | solution.py:63
  26.2 5.2 %all_gather.13 = f32[2,2048]{1,0:T(2,128)S(1)} all-gather(f32[2,512]{1,0:T(2,128)S(1)} %get-tuple-element.5), channel_id=1, replica_groups=mesh['grp'=2,'sp'=4,'tp'=4] {'tp'}, dimensions={1}, use_global_device_ids=true | all-gather | bytes 20480 | tf_op jit(solution)/shard_map/all_gather | solution.py:65
  31.4 5.2 %all_gather.12 = f32[2,2048]{1,0:T(2,128)S(1)} all-gather(f32[2,512]{1,0:T(2,128)S(1)} %get-tuple-element.6), channel_id=1, replica_groups=mesh['grp'=2,'sp'=4,'tp'=4] {'tp'}, dimensions={1}, use_global_device_ids=true | all-gather | bytes 20480 | tf_op jit(solution)/shard_map/all_gather | solution.py:66
  37.9 1.8 %fusion.2 = f32[384]{0:T(512)S(1)} fusion(bf16[384,2048]{1,0:T(8,128)(2,1)} %param.13), kind=kLoop, calls=%fused_computation.10 | loop fusion | flops 2358912 | bytes 1574400 | tf_op jit(solution)/shard_map/reduce_sum | solution.py:30
  39.7 2.1 %fusion.6 = bf16[384,2048]{1,0:T(8,128)(2,1)S(1)} fusion(bf16[384,2048]{1,0:T(8,128)(2,1)} %param.13, f32[2048]{0:T(1024)S(1)} %bitcast.76, f32[2048]{0:T(1024)S(1)} %bitcast.77, f32[2048]{0:T(1024)S(1)} %convert_element_type.62, f32[384]{0:T(512)S(1)} %add_rsqrt_fusion), kind=kLoop, calls=%fused_computation.14 | loop fusion | flops 4718592 | bytes 3171840 | tf_op jit(solution)/shard_map/convert_element_type | solution.py:33
  41.8 2.0 %convolution_convert_fusion.2 = bf16[384,256]{0,1:T(8,128)(2,1)S(1)} fusion(bf16[384,2048]{1,0:T(8,128)(2,1)S(1)} %fusion.6, bf16[2048,256]{1,0:T(8,128)(2,1)} %param.22), kind=kOutput, calls=%fused_computation.28 | convolution fusion | flops 402751488 | bytes 2818048 | tf_op jit(solution)/shard_map/dot_general | solution.py:37
  47.6 5.3 %collective-permute-start = (bf16[4,64,512]{2,1,0:T(8,128)(2,1)}, bf16[4,64,512]{2,1,0:T(8,128)(2,1)}, u32[]{:S(2)}, u32[]{:S(2)}) collective-permute-start(bf16[4,64,512]{2,1,0:T(8,128)(2,1)} %bitcast.3), channel_id=1, source_target_pairs={{0,4},{4,8},{8,12},{1,5},{5,9},{9,13},{2,6},{6,10},{10,14},{3,7},{... | collective-permute-start | bytes 786440 | tf_op jit(solution)/shard_map/ppermute | solution.py:20
  54.0 1.6 convolution_convert_fusion.3
  57.3 2.5 %convolution_convert_fusion = bf16[384,256]{1,0:T(8,128)(2,1)} fusion(bf16[384,2048]{1,0:T(8,128)(2,1)S(1)} %fusion.6, bf16[2048,256]{1,0:T(8,128)(2,1)} %param.21), kind=kOutput, calls=%fused_computation.26 | convolution fusion | flops 402751488 | bytes 2818048 | tf_op jit(solution)/shard_map/dot_general | solution.py:37
  59.7 13.3 %all_gather.14 = bf16[64,512]{1,0:T(8,128)(2,1)S(1)} all-gather(bf16[16,512]{1,0:T(8,128)(2,1)S(1)} %pad_maximum_fusion.2), channel_id=1, replica_groups=mesh['grp'=2,'sp'=4,'tp'=4] {'sp'}, dimensions={0}, use_global_device_ids=true | all-gather | bytes 81920 | tf_op jit(solution)/shard_map/all_gather | solution.py:75
  73.2 30.3 %gather_fusion.1 = f32[4096,4,15]{2,1,0:T(4,128)} fusion(f32[4,15,31]{1,0,2:T(4,128)S(1)} %copy.67, s32[4096]{0:T(1024)S(1)} %broadcast_clamp_fusion), kind=kCustom, calls=%fused_computation.1 | custom fusion | bytes 1982464 | tf_op jit(solution)/shard_map/gather | solution.py:106
  103.5 7.3 %copy.68 = f32[64,64,4,15]{1,0,2,3:T(8,128)S(1)} copy(f32[64,64,4,15]{3,2,1,0:T(4,128)} %bitcast.67) | data formatting | bytes 1966080 | tf_op jit(solution)/shard_map/gather | solution.py:106
  110.8 3.8 %gather_fusion.2 = f32[6,4,8,64,64]{4,3,1,2,0:T(8,128)} fusion(f32[4,15,64,64]{3,2,0,1:T(8,128)S(1)} %bitcast.63, s32[6]{0:T(128)S(1)} %shift-left_bitcast_fusion), kind=kCustom, calls=%fused_computation.2 | custom fusion | bytes 6291552 | tf_op jit(solution)/shard_map/vmap()/gather | solution.py:109
  114.6 6.7 %copy.69 = f32[6,4,8,64,64]{3,4,2,1,0:T(8,128)} copy(f32[6,4,8,64,64]{4,3,1,2,0:T(8,128)} %gather_fusion.2) | data formatting | bytes 6291456 | tf_op jit(solution)/shard_map/vmap()/gather | solution.py:109
  124.4 2.5 %gather_fusion = bf16[6,8,64,512]{3,2,1,0:T(8,128)(2,1)} fusion(bf16[14,64,512]{2,1,0:T(8,128)(2,1)S(1)} %pad_maximum_fusion, s32[6]{0:T(128)S(1)} %shift-left_bitcast_fusion.1), kind=kCustom, calls=%fused_computation | custom fusion | bytes 6291528 | tf_op jit(solution)/shard_map/vmap()/gather | solution.py:94
  126.9 3.4 %fusion.45 = (bf16[6,8,64,256]{3,2,1,0:T(8,128)(2,1)S(1)}, bf16[6,8,64,256]{3,2,1,0:T(8,128)(2,1)}) fusion(bf16[6,8,64,512]{3,2,1,0:T(8,128)(2,1)} %gather_fusion), kind=kLoop, calls=%fused_computation.90 | loop fusion | bytes 6291456 | tf_op jit(solution)/shard_map/slice | solution.py:97
  130.3 5.8 %reshape.185 = bf16[6,8,64,4,64]{4,3,2,1,0:T(4,128)(2,1)} reshape(bf16[6,8,64,256]{3,2,1,0:T(8,128)(2,1)} %get-tuple-element.11) | data formatting | bytes 3145728 | tf_op jit(solution)/shard_map/reshape | solution.py:96
  136.1 2.9 %copy.66 = bf16[6,8,64,4,64]{4,2,1,3,0:T(8,128)(2,1)S(1)} copy(bf16[6,8,64,4,64]{4,3,2,1,0:T(4,128)(2,1)} %reshape.185) | data formatting | bytes 3145728 | tf_op jit(solution)/shard_map/reshape | solution.py:96
  140.6 4.2 %fusion.43 = (f32[6,4,64]{2,1,0:T(4,128)S(1)}, f32[6,4,64,8,64]{2,4,3,1,0:T(8,128)}) fusion(f32[6,4,8,64,64]{3,4,2,1,0:T(8,128)S(1)} %bitcast.65, pred[64,64]{0,1:T(8,128)(4,1)S(1)} %fusion.30, f32[6,4,64,512]{2,3,1,0:S(1)} %fusion.20), kind=kLoop, calls=%fused_computation.89 | loop fusion | flops 3144192 | bytes 9447424 | tf_op jit(solution)/shard_map/reduce_max | solution.py:122
  144.9 3.8 %fusion.1 = f32[6,4,64]{2,1,0:T(4,128)S(1)} fusion(f32[6,4,64,8,64]{2,4,3,1,0:T(8,128)} %get-tuple-element.9, f32[6,4,64]{2,1,0:T(4,128)S(1)} %copy_maximum_fusion), kind=kLoop, calls=%fused_computation.7 | loop fusion | flops 1571328 | bytes 3158016 | tf_op jit(solution)/shard_map/reduce_sum | solution.py:125
  148.7 2.9 %reshape.183 = bf16[6,8,64,4,64]{4,3,2,1,0:T(4,128)(2,1)} reshape(bf16[6,8,64,256]{3,2,1,0:T(8,128)(2,1)S(1)} %get-tuple-element.10) | data formatting | bytes 3145728 | tf_op jit(solution)/shard_map/reshape | solution.py:97
  151.8 5.4 %fusion.9 = f32[6,64,4,64]{1,3,2,0:T(8,128)S(1)} fusion(f32[6,4,64,8,64]{2,4,3,1,0:T(8,128)} %get-tuple-element.9, f32[6,4,64]{2,1,0:T(4,128)S(1)} %copy_add_fusion, f32[6,4,64]{2,1,0:T(4,128)S(1)} %copy_maximum_fusion, bf16[6,8,64,4,64]{4,3,2,1,0:T(4,128)(2,1)} %reshape.183), kind=kOutput, calls=%fused_computation.17 | convolution fusion | flops 103022592 | bytes 5124096 | tf_op jit(solution)/shard_map/rhcij,rijhd->rchd/dot_general | solution.py:128
  158.0 8.6 %all_gather.15 = bf16[384,1024]{1,0:T(8,128)(2,1)S(1)} all-gather(bf16[384,256]{1,0:T(8,128)(2,1)S(1)} %reshape.188), channel_id=1, replica_groups=mesh['grp'=2,'sp'=4,'tp'=4] {'tp'}, dimensions={1}, use_global_device_ids=true | all-gather | bytes 983040 | tf_op jit(solution)/shard_map/all_gather | solution.py:136
  166.6 2.3 %fusion.16 = bf16[384,512]{1,0:T(8,128)(2,1)} fusion(bf16[384,1024]{1,0:T(8,128)(2,1)S(1)} %all_gather.15, bf16[1024,512]{1,0:T(8,128)(2,1)S(1)} %copy-done, f32[512]{0:T(512)S(1)} %copy-done.5, bf16[384,2048]{1,0:T(8,128)(2,1)} %param.13, s32[]{:T(128)S(6)} %select_n.37), kind=kOutput, calls=%fused_computation.25 | convolution fusion | flops 403439616 | bytes 2623492 | tf_op jit(solution)/shard_map/dot_general | solution.py:135
  (65 shorter events, 18.9 us)
Async XLA Ops:
  0.0 166.6 %copy-start = (bf16[1024,512]{1,0:T(8,128)(2,1)S(1)}, bf16[1024,512]{1,0:T(8,128)(2,1)}, u32[]{:S(2)}) copy-start(bf16[1024,512]{1,0:T(8,128)(2,1)} %param.25) | copy-start | bytes 3145732
  39.7 4.2 %copy-start.1 = (bf16[2048,256]{1,0:T(8,128)(2,1)S(1)}, bf16[2048,256]{1,0:T(8,128)(2,1)}, u32[]{:S(2)}) copy-start(bf16[2048,256]{1,0:T(8,128)(2,1)} %param.23) | copy-start | bytes 3145732
  45.5 77.8 %collective-permute-start.1 = (bf16[4,64,512]{2,1,0:T(8,128)(2,1)}, bf16[4,64,512]{2,1,0:T(8,128)(2,1)}, u32[]{:S(2)}, u32[]{:S(2)}) collective-permute-start(bf16[4,64,512]{2,1,0:T(8,128)(2,1)} %bitcast.70), channel_id=1, source_target_pairs={{4,0},{8,4},{12,8},{5,1},{9,5},{13,9},{6,2},{10,6},{14,10},{7,3},{... | collective-permute-start | bytes 786440 | tf_op jit(solution)/shard_map/ppermute | solution.py:23
  47.6 75.6 %collective-permute-start = (bf16[4,64,512]{2,1,0:T(8,128)(2,1)}, bf16[4,64,512]{2,1,0:T(8,128)(2,1)}, u32[]{:S(2)}, u32[]{:S(2)}) collective-permute-start(bf16[4,64,512]{2,1,0:T(8,128)(2,1)} %bitcast.3), channel_id=1, source_target_pairs={{0,4},{4,8},{8,12},{1,5},{5,9},{9,13},{2,6},{6,10},{10,14},{3,7},{... | collective-permute-start | bytes 786440 | tf_op jit(solution)/shard_map/ppermute | solution.py:20
  54.0 19.1 %copy-start.4 = (f32[4,15,31]{2,0,1:T(4,128)S(1)}, f32[4,15,31]{2,0,1:T(4,128)}, u32[]{:S(2)}) copy-start(f32[4,15,31]{2,0,1:T(4,128)} %param.24) | copy-start | bytes 22324
  114.6 6.9 %copy-start.3 = (bf16[384,256]{1,0:T(8,128)(2,1)S(1)}, bf16[384,256]{1,0:T(8,128)(2,1)}, u32[]{:S(2)}) copy-start(bf16[384,256]{1,0:T(8,128)(2,1)} %convolution_convert_fusion) | copy-start | bytes 589828
  136.1 3.9 %slice-start = ((s8[6291456]{0:T(1024)(128)(4,1)}), s8[4194304]{0:T(1024)(128)(4,1)S(1)}, s32[]{:S(2)}) async-start(s8[6291456]{0:T(1024)(128)(4,1)} %bitcast.64), calls=%async_computation | async-start | bytes 8388608
  138.9 1.7 slice-start.1
  148.7 2.9 %copy-start.2 = (f32[6,4,64,64]{2,3,0,1:T(8,128)S(1)}, f32[6,4,64,64]{2,3,0,1:T(8,128)}, u32[]{:S(2)}) copy-start(f32[6,4,64,64]{2,3,0,1:T(8,128)} %get-tuple-element.21) | copy-start | bytes 1179652
  157.2 9.4 %copy-start.5 = (f32[512]{0:T(512)S(1)}, f32[512]{0:T(512)}, u32[]{:S(2)}) copy-start(f32[512]{0:T(512)} %get-tuple-element.7) | copy-start | bytes 6148
where the time goes:
time: 170 us; the launch traced here: 169 us
  local copies, waits for them, and re-layouts  69.1 us (41%)
  blocking collectives  53.3 us (31%)
  matrix products  22.4 us (13%)
  other arithmetic  17.2 us (10%)
  starting transfers between devices  6.55 us (4%)
    gather x2, local copies, waits for them, and re-layouts, local(): table_cols = offset_bias[:, :, col_offset]  37.6 us
    psum x1, blocking collectives, local(): lax.psum((part_shift, part_scale, part_gate), 'sp')  21 us
    all_gather x1, blocking collectives, local(): lax.all_gather(jnp.concatenate([project(ctx_normed, w_key), project(ctx_n...  13.3 us
    gather x2, local copies, waits for them, and re-layouts, local(): lax.dynamic_slice_in_dim(table_cols, offset_row, WIN_H, 1)  10.4 us
    reshape x2, local copies, waits for them, and re-layouts, local(): windows[..., :head_width]  8.64 us
    all_gather x1, blocking collectives, local(): lax.all_gather(attended, 'tp', axis=1, tiled=True)  8.6 us
    dot_general x5, matrix products, project(): jnp.dot(inputs, weight, preferred_element_type=jnp.float32)  8.4 us
    dot_general x1, matrix products, local(): jnp.einsum('rhcij,rijhd->rchd', win_weights, value_window, preferred_elem...  5.39 us
  transfers between devices with their start and end apart: 2, of which 0 were waited for; matrix products, arithmetic and copies ran while one was open for 34% of the time, Pallas kernels for 0%

commit v1 on v0

v1 whole, which is shorter than its diff:
```python
import functools

import jax
import jax.numpy as jnp
from jax import lax
from jax.experimental import pallas as pl
from jax.experimental.pallas import tpu as pltpu
from jax.sharding import PartitionSpec as P

HEAD_DIM = 64
GRID_W = 64
WIN_H = 8
WIN_W = 16
EPSILON = 1e-06
F32 = jnp.float32
BF16 = jnp.bfloat16
MESH = pl.DeviceIdType.MESH
LOW = WIN_H // 2
HIGH = WIN_H - 1 - LOW
SPAN = WIN_H + 1
TABLE = 2 * WIN_H
PAIR = 2 * GRID_W


def silu(values):
    floats = values.astype(F32)
    return (floats / (1.0 + jnp.exp(-floats))).astype(BF16).astype(F32)


def kernel(
    n_sp,
    n_tp,
    cond_ref,
    ctxv_ref,
    gain_ref,
    context_ref,
    bias_ref,
    lat_hbm,
    wsh_hbm,
    wsc_hbm,
    wga_hbm,
    wq_hbm,
    wk_hbm,
    wv_hbm,
    wo_hbm,
    out_ref,
    lat,
    wmod,
    wqkv,
    wo,
    part,
    mod,
    inv_ref,
    normed,
    qbuf,
    kv,
    table,
    att,
    load_sem,
    part_send,
    part_recv,
    mod_send,
    mod_recv,
    ctx_send,
    ctx_recv,
    halo_send,
    halo_recv,
    att_send,
    att_recv,
):
    sp = lax.axis_index("sp")
    tp = lax.axis_index("tp")
    tokens, width = lat.shape
    head_width = wqkv.shape[2]
    cols = wmod.shape[2]
    ctx_own = context_ref.shape[0]
    rows_dev = tokens // GRID_W
    pairs = rows_dev // 2
    groups = head_width // 128
    n_ctx = ctx_own * n_sp
    own0 = LOW * GRID_W
    high0 = own0 + tokens
    ctx0 = high0 + HIGH * GRID_W

    barrier = pltpu.get_barrier_semaphore()
    for k in range(1, n_sp):
        pl.semaphore_signal(barrier, 1, device_id={"sp": lax.rem(sp + k, n_sp)}, device_id_type=MESH)
    for k in range(1, n_tp):
        pl.semaphore_signal(barrier, 1, device_id={"tp": lax.rem(tp + k, n_tp)}, device_id_type=MESH)

    loads = [
        pltpu.make_async_copy(src, dst, load_sem.at[i])
        for i, (src, dst) in enumerate(
            [
                (wsh_hbm, wmod.at[0]),
                (wsc_hbm, wmod.at[1]),
                (wga_hbm, wmod.at[2]),
                (lat_hbm, lat),
                (wk_hbm, wqkv.at[1]),
                (wv_hbm, wqkv.at[2]),
                (wq_hbm, wqkv.at[0]),
                (wo_hbm, wo),
            ]
        )
    ]
    for load in loads:
        load.start()

    row = lax.broadcasted_iota(jnp.int32, (16, cond_ref.shape[1]), 0)
    cond_act = jnp.broadcast_to(silu(cond_ref[...]), row.shape)
    ctx_act = jnp.broadcast_to(silu(ctxv_ref[...]), row.shape)
    total = None
    for m in range(3):
        acts = jnp.where(row == m, cond_act, 0.0)
        if m < 2:
            acts = jnp.where(row == m + 3, ctx_act, acts)
        loads[m].wait()
        term = jnp.dot(acts.astype(BF16), wmod[m], preferred_element_type=F32)
        total = term if total is None else total + term
    part[sp] = total[:8]

    pl.semaphore_wait(barrier, n_sp + n_tp - 2)

    def part_copy(slot, peer):
        return pltpu.make_async_remote_copy(
            src_ref=part.at[slot],
            dst_ref=part.at[slot],
            send_sem=part_send.at[peer],
            recv_sem=part_recv.at[slot],
            device_id={"sp": peer},
            device_id_type=MESH,
        )

    sp_peers = [lax.rem(sp + k, n_sp) for k in range(1, n_sp)]
    tp_peers = [lax.rem(tp + k, n_tp) for k in range(1, n_tp)]
    part_sends = [part_copy(sp, peer) for peer in sp_peers]
    for copy in part_sends:
        copy.start()

    loads[3].wait()
    for r in range(rows_dev):
        block = lat[r * GRID_W : (r + 1) * GRID_W, :].astype(F32)
        mean = jnp.mean(block * block, axis=-1, keepdims=True)
        inv_ref[r * GRID_W : (r + 1) * GRID_W, :] = jnp.broadcast_to(
            lax.rsqrt(mean + EPSILON), (GRID_W, 128)
        )
    block = context_ref[...].astype(F32)
    inv_ctx = lax.rsqrt(jnp.mean(block * block, axis=-1, keepdims=True) + EPSILON)

    key_col = lax.broadcasted_iota(jnp.int32, (GRID_W, PAIR), 0)
    lane = lax.broadcasted_iota(jnp.int32, (GRID_W, PAIR), 1)
    query_col = jnp.where(lane >= GRID_W, lane - GRID_W, lane)
    first_col = jnp.clip(query_col - WIN_W // 2, 0, GRID_W - WIN_W)
    inside = (key_col >= first_col) & (key_col < first_col + WIN_W)
    for g in range(groups):
        for hh in range(2):

            def expand(d, _, g=g, hh=hh):
                line = bias_ref[2 * g + hh, pl.ds(d, 1), :]
                turned = pltpu.roll(
                    jnp.broadcast_to(line, (GRID_W, PAIR)), 0, 1, stride=1, stride_axis=0
                )
                table[g, d, :, hh * PAIR : (hh + 1) * PAIR] = jnp.where(inside, turned, -jnp.inf)
                return 0

            lax.fori_loop(0, TABLE, expand, 0)

    @pl.when(sp == 0)
    def _():
        kv[0:own0, :] = jnp.zeros((own0, 2 * head_width), BF16)

    @pl.when(sp == n_sp - 1)
    def _():
        kv[high0:ctx0, :] = jnp.zeros((ctx0 - high0, 2 * head_width), BF16)

    for peer in sp_peers:
        part_copy(peer, peer).wait_recv()
    summed = part[0]
    for k in range(1, n_sp):
        summed = summed + part[k]
    mod[tp] = summed

    def mod_copy(slot, peer):
        return pltpu.make_async_remote_copy(
            src_ref=mod.at[slot],
            dst_ref=mod.at[slot],
            send_sem=mod_send.at[peer],
            recv_sem=mod_recv.at[slot],
            device_id={"tp": peer},
            device_id_type=MESH,
        )

    mod_sends = [mod_copy(tp, peer) for peer in tp_peers]
    for copy in mod_sends:
        copy.start()
    for copy in part_sends:
        copy.wait_send()
    for peer in tp_peers:
        mod_copy(peer, peer).wait_recv()

    for t in range(n_tp):
        span = slice(t * cols, (t + 1) * cols)
        gain = gain_ref[:, span].astype(F32)
        vectors = mod[t]
        factor, shift = gain * (1.0 + vectors[1:2]), vectors[0:1]
        ctx_factor, ctx_shift = gain * (1.0 + vectors[4:5]), vectors[3:4]
        for r in range(rows_dev):
            rows = slice(r * GRID_W, (r + 1) * GRID_W)
            normed[rows, span] = (
                lat[rows, span].astype(F32) * inv_ref[rows, 0:1] * factor + shift
            ).astype(BF16)
        normed[tokens:, span] = (
            context_ref[:, span].astype(F32) * inv_ctx * ctx_factor + ctx_shift
        ).astype(BF16)

    ctx_own_rows = pl.ds(pl.multiple_of(ctx0 + sp * ctx_own, ctx_own), ctx_own)
    for i in range(2):
        loads[4 + i].wait()
        product = jnp.dot(normed[...], wqkv[1 + i], preferred_element_type=F32).astype(BF16)
        lanes = slice(i * head_width, (i + 1) * head_width)
        kv[own0:high0, lanes] = product[:tokens]
        kv[ctx_own_rows, lanes] = product[tokens:]

    up = pltpu.make_async_remote_copy(
        src_ref=kv.at[pl.ds(high0 - own0, own0)],
        dst_ref=kv.at[pl.ds(0, own0)],
        send_sem=halo_send.at[0],
        recv_sem=halo_recv.at[0],
        device_id={"sp": lax.rem(sp + 1, n_sp)},
        device_id_type=MESH,
    )
    down = pltpu.make_async_remote_copy(
        src_ref=kv.at[pl.ds(own0, HIGH * GRID_W)],
        dst_ref=kv.at[pl.ds(high0, HIGH * GRID_W)],
        send_sem=halo_send.at[1],
        recv_sem=halo_recv.at[1],
        device_id={"sp": lax.rem(sp + n_sp - 1, n_sp)},
        device_id_type=MESH,
    )

    def ctx_copy(slot, peer):
        rows = pl.ds(pl.multiple_of(ctx0 + slot * ctx_own, ctx_own), ctx_own)
        return pltpu.make_async_remote_copy(
            src_ref=kv.at[rows],
            dst_ref=kv.at[rows],
            send_sem=ctx_send.at[peer],
            recv_sem=ctx_recv.at[slot],
            device_id={"sp": peer},
            device_id_type=MESH,
        )

    ctx_sends = [ctx_copy(sp, peer) for peer in sp_peers]
    for copy in ctx_sends:
        copy.start()

    @pl.when(sp < n_sp - 1)
    def _():
        up.start()

    @pl.when(sp > 0)
    def _():
        down.start()

    loads[6].wait()
    qbuf[...] = (
        jnp.dot(normed[:tokens], wqkv[0], preferred_element_type=F32) * HEAD_DIM ** (-0.5)
    ).astype(BF16)

    for copy in mod_sends:
        copy.wait_send()
    for peer in sp_peers:
        ctx_copy(peer, peer).wait_recv()

    @pl.when(sp > 0)
    def _():
        up.wait_recv()

    @pl.when(sp < n_sp - 1)
    def _():
        down.wait_recv()

    partner = tp + 1 - 2 * lax.rem(tp, 2)
    chips = n_tp // 2
    others = [lax.rem(tp + 2 * k, n_tp) for k in range(1, chips)]

    def att_copy(b, slot, peer, k):
        rows = pl.ds(b * PAIR, PAIR)
        return pltpu.make_async_remote_copy(
            src_ref=att.at[slot, rows],
            dst_ref=att.at[slot, rows],
            send_sem=att_send.at[b, k],
            recv_sem=att_recv.at[b, slot],
            device_id={"tp": peer},
            device_id_type=MESH,
        )

    lane_two = lax.broadcasted_iota(jnp.int32, (1, 2 * PAIR), 1)
    late = lax.rem(lane_two, PAIR) >= GRID_W
    lane_q = lax.broadcasted_iota(jnp.int32, (PAIR, 128), 1)
    grid_rows = rows_dev * n_sp
    row_base = sp * rows_dev

    def start_of(i):
        return jnp.clip(row_base + i - WIN_H // 2, 0, grid_rows - WIN_H) - row_base + LOW

    att_sends = []
    for b in range(pairs):
        i = 2 * b
        start = start_of(i)
        moved = start_of(i + 1) - start
        first = start - i + (WIN_H - 1 - LOW)
        mask_low = jnp.where(late & (moved == 1), -jnp.inf, 0.0)
        mask_high = jnp.where(late & (moved == 1), 0.0, -jnp.inf)
        window = pl.ds(pl.multiple_of(start * GRID_W, GRID_W), SPAN * GRID_W)
        for g in range(groups):
            lanes = slice(g * 128, (g + 1) * 128)
            vlanes = slice(head_width + g * 128, head_width + (g + 1) * 128)
            query = qbuf[b * PAIR : (b + 1) * PAIR, lanes]
            zero = jnp.zeros_like(query)
            stacked = jnp.concatenate(
                [jnp.where(lane_q < HEAD_DIM, query, zero), jnp.where(lane_q < HEAD_DIM, zero, query)],
                axis=0,
            )
            nt = (((1,), (1,)), ((), ()))
            tn = (((0,), (0,)), ((), ()))
            scores = lax.dot_general(kv[window, lanes], stacked, nt, preferred_element_type=F32)
            ctx_scores = lax.dot_general(
                kv[ctx0 : ctx0 + n_ctx, lanes], stacked, nt, preferred_element_type=F32
            )
            bias = table[g, pl.ds(first, SPAN)].reshape(SPAN * GRID_W, 2 * PAIR)
            scores = scores + bias
            head = scores[:GRID_W] + mask_low
            body = scores[GRID_W : WIN_H * GRID_W]
            tail = scores[WIN_H * GRID_W :] + mask_high
            pieces = [head, body, tail, ctx_scores]
            highest = functools.reduce(
                jnp.maximum, [jnp.max(piece, axis=0, keepdims=True) for piece in pieces]
            )
            pieces = [jnp.exp(piece - highest) for piece in pieces]
            sums = functools.reduce(
                jnp.add, [jnp.sum(piece, axis=0, keepdims=True) for piece in pieces]
            )
            weights = jnp.concatenate([piece.astype(BF16) for piece in pieces[:3]], axis=0)
            result = lax.dot_general(kv[window, vlanes], weights, tn, preferred_element_type=F32)
            result = result + lax.dot_general(
                kv[ctx0 : ctx0 + n_ctx, vlanes], pieces[3].astype(BF16), tn, preferred_element_type=F32
            )
            result = result / sums
            both = jnp.concatenate(
                [result[:HEAD_DIM, :PAIR], result[HEAD_DIM:, PAIR:]], axis=0
            )
            att[tp, b * PAIR : (b + 1) * PAIR, lanes] = both.T.astype(BF16)
        sends = [att_copy(b, tp, partner, 0)]
        sends += [att_copy(b, tp, peer, 1 + k) for k, peer in enumerate(others)]
        for copy in sends[1:] + sends[:1]:
            copy.start()
        att_sends += sends

    for b in range(pairs):
        for k, peer in enumerate(others):
            att_copy(b, peer, peer, 1 + k).wait_recv()
            forward = att_copy(b, peer, partner, chips + k)
            forward.start()
            att_sends.append(forward)

    loads[7].wait()
    gate = mod[tp][2:3]
    own_cols = pl.ds(pl.multiple_of(tp * cols, cols), cols)
    for b in range(pairs):
        rows = slice(b * PAIR, (b + 1) * PAIR)
        att_copy(b, partner, partner, 0).wait_recv()
        for k, peer in enumerate(others):
            source = peer + 1 - 2 * lax.rem(peer, 2)
            att_copy(b, source, partner, 0).wait_recv()
        branch = None
        for t in range(n_tp):
            term = jnp.dot(
                att[t, rows],
                wo[t * head_width : (t + 1) * head_width, :],
                preferred_element_type=F32,
            )
            branch = term if branch is None else branch + term
        out_ref[rows, :] = (lat[rows, own_cols].astype(F32) + gate * branch).astype(BF16)

    for copy in ctx_sends + att_sends:
        copy.wait_send()

    @pl.when(sp < n_sp - 1)
    def _():
        up.wait_send()

    @pl.when(sp > 0)
    def _():
        down.wait_send()


def local(
    n_sp,
    n_tp,
    latent,
    conditioning,
    context,
    ctx_vector,
    w_shift,
    w_scale,
    w_gate,
    norm_gain,
    w_query,
    w_key,
    w_value,
    offset_bias,
    w_out,
):
    tokens, width = latent.shape
    head_width = w_query.shape[1]
    cols = w_shift.shape[1]
    heads = head_width // HEAD_DIM
    ctx_own = context.shape[0]
    key_rows = tokens + (LOW + HIGH) * GRID_W + ctx_own * n_sp
    rows_dev = tokens // GRID_W
    pairs = rows_dev // 2
    chips = n_tp // 2

    turned = offset_bias[:, :, ::-1]
    early = jnp.pad(turned, ((0, 0), (0, 1), (0, 0)))
    later = jnp.pad(turned, ((0, 0), (1, 0), (0, 0)))
    reach = WIN_W - 1
    gap = jnp.zeros((heads, TABLE, GRID_W - 2 * reach - 1), F32)
    lines = jnp.concatenate(
        [early[..., reach:], gap, later, gap, early[..., :reach]], axis=-1
    )

    vmem = pl.BlockSpec(memory_space=pltpu.VMEM)
    anywhere = pl.BlockSpec(memory_space=pl.ANY)
    dma = pltpu.SemaphoreType.DMA
    return pl.pallas_call(
        functools.partial(kernel, n_sp, n_tp),
        out_shape=jax.ShapeDtypeStruct((tokens, cols), BF16),
        in_specs=[vmem] * 5 + [anywhere] * 8,
        out_specs=vmem,
        scratch_shapes=[
            pltpu.VMEM((tokens, width), BF16),
            pltpu.VMEM((3,) + w_shift.shape, BF16),
            pltpu.VMEM((3,) + w_query.shape, BF16),
            pltpu.VMEM(w_out.shape, BF16),
            pltpu.VMEM((n_sp, 8, cols), F32),
            pltpu.VMEM((n_tp, 8, cols), F32),
            pltpu.VMEM((tokens, 128), F32),
            pltpu.VMEM((tokens + ctx_own, width), BF16),
            pltpu.VMEM((tokens, head_width), BF16),
            pltpu.VMEM((key_rows, 2 * head_width), BF16),
            pltpu.VMEM((heads // 2, TABLE, GRID_W, 2 * PAIR), F32),
            pltpu.VMEM((n_tp, tokens, head_width), BF16),
            dma((8,)),
            dma((n_sp,)),
            dma((n_sp,)),
            dma((n_tp,)),
            dma((n_tp,)),
            dma((n_sp,)),
            dma((n_sp,)),
            dma((2,)),
            dma((2,)),
            dma((pairs, 2 * chips)),
            dma((pairs, n_tp)),
        ],
        compiler_params=pltpu.CompilerParams(
            collective_id=0, has_side_effects=True, vmem_limit_bytes=48 * 1024 * 1024
        ),
    )(
        conditioning.reshape(1, -1),
        ctx_vector.reshape(1, -1),
        norm_gain.reshape(1, -1),
        context,
        lines,
        latent,
        w_shift,
        w_scale,
        w_gate,
        w_query,
        w_key,
        w_value,
        w_out,
    )


def solution(mesh):
    return jax.shard_map(
        functools.partial(local, mesh.shape["sp"], mesh.shape["tp"]),
        mesh=mesh,
        in_specs=(
            P(("grp", "sp"), None),
            P(("grp", "sp")),
            P(("grp", "sp"), None),
            P("sp"),
            P("sp", "tp"),
            P("sp", "tp"),
            P("sp", "tp"),
            P(),
            P(None, "tp"),
            P(None, "tp"),
            P(None, "tp"),
            P("tp", None, None),
            P(None, "tp"),
        ),
        out_specs=P(("grp", "sp"), "tp"),
        check_vma=False,
    )
```

time: 170 us -> 43.8 us (0.26)
  the two profiles are of different devices: /device:TPU:0 before, /device:TPU:9 now
where the time goes in v1:
time: 43.8 us; the launch traced here: 43.3 us
  Pallas kernels  31.8 us (73%)
  local copies, waits for them, and re-layouts  11.5 us (26%)
    pallas_call x1, Pallas kernels, local(): pl.pallas_call(functools.partial(kernel, n_sp, n_tp), out_shape=jax.Shape...  31.8 us
    unnamed x16, local copies, waits for them, and re-layouts  9.14 us

profile of v1, /device:TPU:9, one launch (start us, length us, event | category | flops | bytes accessed | tf_op | source)
XLA Modules:
  0.0 43.3 jit_solution(6667040388430014278)
XLA Ops:
  0.0 0.7 %reshape.9.cond_ref = bf16[1,512]{1,0:T(2,128)(2,1)S(1)} reshape(bf16[512]{0:T(512)(128)(2,1)} %param.14) | data formatting | bytes 2048 | tf_op jit(solution)/shard_map/reshape | solution.py:470
  0.7 0.7 %reshape.10.ctxv_ref = bf16[1,512]{1,0:T(2,128)(2,1)S(1)} reshape(bf16[512]{0:T(512)(128)(2,1)} %param.16) | data formatting | bytes 2048 | tf_op jit(solution)/shard_map/reshape | solution.py:471
  1.4 0.7 %reshape.11.gain_ref = bf16[1,2048]{1,0:T(2,128)(2,1)S(1)} reshape(bf16[2048]{0:T(1024)(128)(2,1)} %param.20) | data formatting | bytes 8192 | tf_op jit(solution)/shard_map/reshape | solution.py:472
  2.1 0.8 %copy.14 = f32[4,15,31]{2,1,0:T(8,128)S(1)} copy(f32[4,15,31]{2,0,1:T(4,128)} %param.24) | data formatting | bytes 14880 | tf_op args[11]
  2.8 0.1 rev.3
  2.9 0.1 pad_slice_fusion.1
  3.0 0.1 concatenate.3.bias_ref
  3.1 0.0 copy-start
  3.1 1.2 %copy-done = bf16[2048,256]{1,0:T(8,128)(2,1)S(1)} copy-done((bf16[2048,256]{1,0:T(8,128)(2,1)S(1)}, bf16[2048,256]{1,0:T(8,128)(2,1)}, u32[]{:S(2)}) %copy-start) | copy-done | bytes 1048600
  4.3 0.0 copy-start.1
  4.3 1.2 %copy-done.1 = bf16[2048,256]{1,0:T(8,128)(2,1)S(1)} copy-done((bf16[2048,256]{1,0:T(8,128)(2,1)S(1)}, bf16[2048,256]{1,0:T(8,128)(2,1)}, u32[]{:S(2)}) %copy-start.1) | copy-done | bytes 1048600
  5.6 0.0 copy-start.2
  5.6 1.2 %copy-done.2 = bf16[2048,256]{1,0:T(8,128)(2,1)S(1)} copy-done((bf16[2048,256]{1,0:T(8,128)(2,1)S(1)}, bf16[2048,256]{1,0:T(8,128)(2,1)}, u32[]{:S(2)}) %copy-start.2) | copy-done | bytes 1048600
  6.8 0.0 copy-start.3
  6.8 1.0 %copy-done.3 = bf16[512,512]{1,0:T(8,128)(2,1)S(1)} copy-done((bf16[512,512]{1,0:T(8,128)(2,1)S(1)}, bf16[512,512]{1,0:T(8,128)(2,1)}, u32[]{:S(2)}) %copy-start.3) | copy-done | bytes 524312
  7.8 0.0 copy-start.4
  7.8 1.0 %copy-done.4 = bf16[512,512]{1,0:T(8,128)(2,1)S(1)} copy-done((bf16[512,512]{1,0:T(8,128)(2,1)S(1)}, bf16[512,512]{1,0:T(8,128)(2,1)}, u32[]{:S(2)}) %copy-start.4) | copy-done | bytes 524312
  8.9 0.0 copy-start.5
  8.9 1.0 %copy-done.5 = bf16[512,512]{1,0:T(8,128)(2,1)S(1)} copy-done((bf16[512,512]{1,0:T(8,128)(2,1)S(1)}, bf16[512,512]{1,0:T(8,128)(2,1)}, u32[]{:S(2)}) %copy-start.5) | copy-done | bytes 524312
  9.9 0.0 copy-start.6
  9.9 0.8 %copy-done.6 = bf16[16,2048]{1,0:T(8,128)(2,1)S(1)} copy-done((bf16[16,2048]{1,0:T(8,128)(2,1)S(1)}, bf16[16,2048]{1,0:T(8,128)(2,1)}, u32[]{:S(2)}) %copy-start.6) | copy-done | bytes 65560
  10.8 31.8 %shard_map.127 = bf16[384,512]{1,0:T(8,128)(2,1)S(1)} custom-call(bf16[1,512]{1,0:T(2,128)(2,1)S(1)} %reshape.9.cond_ref, bf16[1,512]{1,0:T(2,128)(2,1)S(1)} %reshape.10.ctxv_ref, bf16[1,2048]{1,0:T(2,128)(2,1)S(1)} %reshape.11.gain_ref, bf16[16,2048]{1,0:T(8,128)(2,1)S(1)} %copy-done.6, f32[4,16,128]{2,1,0:T(8,128)S(1)} %concatenate.3.bias_ref, ...), custom_call_target="tpu_custom_call" | custom-call | tf_op jit(solution)/shard_map/pallas_call | solution.py:436
  42.5 0.7 %copy.16 = bf16[384,512]{1,0:T(8,128)(2,1)} copy(bf16[384,512]{1,0:T(8,128)(2,1)S(1)} %shard_map.127) | data formatting | bytes 786432
  (3 shorter events, 0.0 us)
Async XLA Ops:
  3.1 1.2 %copy-start = (bf16[2048,256]{1,0:T(8,128)(2,1)S(1)}, bf16[2048,256]{1,0:T(8,128)(2,1)}, u32[]{:S(2)}) copy-start(bf16[2048,256]{1,0:T(8,128)(2,1)} %wq_hbm.1) | copy-start | bytes 3145732
  4.3 1.2 %copy-start.1 = (bf16[2048,256]{1,0:T(8,128)(2,1)S(1)}, bf16[2048,256]{1,0:T(8,128)(2,1)}, u32[]{:S(2)}) copy-start(bf16[2048,256]{1,0:T(8,128)(2,1)} %wk_hbm.1) | copy-start | bytes 3145732
  5.6 1.2 %copy-start.2 = (bf16[2048,256]{1,0:T(8,128)(2,1)S(1)}, bf16[2048,256]{1,0:T(8,128)(2,1)}, u32[]{:S(2)}) copy-start(bf16[2048,256]{1,0:T(8,128)(2,1)} %wv_hbm.1) | copy-start | bytes 3145732
  6.8 1.0 %copy-start.3 = (bf16[512,512]{1,0:T(8,128)(2,1)S(1)}, bf16[512,512]{1,0:T(8,128)(2,1)}, u32[]{:S(2)}) copy-start(bf16[512,512]{1,0:T(8,128)(2,1)} %wsh_hbm.1) | copy-start | bytes 1572868
  7.8 1.0 %copy-start.4 = (bf16[512,512]{1,0:T(8,128)(2,1)S(1)}, bf16[512,512]{1,0:T(8,128)(2,1)}, u32[]{:S(2)}) copy-start(bf16[512,512]{1,0:T(8,128)(2,1)} %wsc_hbm.1) | copy-start | bytes 1572868
  8.9 1.0 %copy-start.5 = (bf16[512,512]{1,0:T(8,128)(2,1)S(1)}, bf16[512,512]{1,0:T(8,128)(2,1)}, u32[]{:S(2)}) copy-start(bf16[512,512]{1,0:T(8,128)(2,1)} %wga_hbm.1) | copy-start | bytes 1572868
  9.9 0.8 %copy-start.6 = (bf16[16,2048]{1,0:T(8,128)(2,1)S(1)}, bf16[16,2048]{1,0:T(8,128)(2,1)}, u32[]{:S(2)}) copy-start(bf16[16,2048]{1,0:T(8,128)(2,1)} %context_ref.1) | copy-start | bytes 196612

commit v2 on v1

--- a/solution.py
+++ b/solution.py
@@ -30,11 +30,11 @@
 def kernel(
     n_sp,
     n_tp,
-    cond_ref,
-    ctxv_ref,
-    gain_ref,
-    context_ref,
-    bias_ref,
+    cond_hbm,
+    ctxv_hbm,
+    gain_hbm,
+    context_hbm,
+    bias_hbm,
     lat_hbm,
     wsh_hbm,
     wsc_hbm,
@@ -44,6 +44,12 @@
     wv_hbm,
     wo_hbm,
     out_ref,
+    cond_ref,
+    ctxv_ref,
+    gain_ref,
+    context_ref,
+    bias_ref,
+    lines,
     lat,
     wmod,
     wqkv,
@@ -100,15 +106,22 @@
                 (wv_hbm, wqkv.at[2]),
                 (wq_hbm, wqkv.at[0]),
                 (wo_hbm, wo),
+                (cond_hbm, cond_ref),
+                (ctxv_hbm, ctxv_ref),
+                (bias_hbm, bias_ref),
+                (context_hbm, context_ref),
+                (gain_hbm, gain_ref),
             ]
         )
     ]
-    for load in loads:
+    for load in loads[8:10] + loads[:3] + loads[10:] + loads[3:8]:
         load.start()
-
-    row = lax.broadcasted_iota(jnp.int32, (16, cond_ref.shape[1]), 0)
-    cond_act = jnp.broadcast_to(silu(cond_ref[...]), row.shape)
-    ctx_act = jnp.broadcast_to(silu(ctxv_ref[...]), row.shape)
+    for load in loads[8:10]:
+        load.wait()
+
+    row = lax.broadcasted_iota(jnp.int32, (16, cond_ref.shape[0]), 0)
+    cond_act = jnp.broadcast_to(silu(cond_ref[...].reshape(1, -1)), row.shape)
+    ctx_act = jnp.broadcast_to(silu(ctxv_ref[...].reshape(1, -1)), row.shape)
     total = None
     for m in range(3):
         acts = jnp.where(row == m, cond_act, 0.0)
@@ -137,6 +150,8 @@
     for copy in part_sends:
         copy.start()
 
+    for load in loads[10:]:
+        load.wait()
     loads[3].wait()
     for r in range(rows_dev):
         block = lat[r * GRID_W : (r + 1) * GRID_W, :].astype(F32)
@@ -152,11 +167,22 @@
     query_col = jnp.where(lane >= GRID_W, lane - GRID_W, lane)
     first_col = jnp.clip(query_col - WIN_W // 2, 0, GRID_W - WIN_W)
     inside = (key_col >= first_col) & (key_col < first_col + WIN_W)
+    offsets, reach = 2 * WIN_W - 1, WIN_W - 1
+    source = lax.broadcasted_iota(jnp.int32, (offsets, PAIR), 0)
+    target = lax.broadcasted_iota(jnp.int32, (offsets, PAIR), 1)
+    early = (lax.rem(target + reach, PAIR) == offsets - 1 - source).astype(F32)
+    later = (target - GRID_W + reach == offsets - 1 - source).astype(F32)
+    lines[...] = jnp.zeros_like(lines)
+    for h in range(2 * groups):
+        exact = lax.Precision.HIGHEST
+        block = bias_ref[:, h, :]
+        lines[h, : TABLE - 1] = jnp.dot(block, early, precision=exact, preferred_element_type=F32)
+        lines[h, 1:] += jnp.dot(block, later, precision=exact, preferred_element_type=F32)
     for g in range(groups):
         for hh in range(2):
 
             def expand(d, _, g=g, hh=hh):
-                line = bias_ref[2 * g + hh, pl.ds(d, 1), :]
+                line = lines[2 * g + hh, pl.ds(d, 1), :]
                 turned = pltpu.roll(
                     jnp.broadcast_to(line, (GRID_W, PAIR)), 0, 1, stride=1, stride_axis=0
                 )
@@ -200,7 +226,7 @@
 
     for t in range(n_tp):
         span = slice(t * cols, (t + 1) * cols)
-        gain = gain_ref[:, span].astype(F32)
+        gain = gain_ref[span].astype(F32).reshape(1, -1)
         vectors = mod[t]
         factor, shift = gain * (1.0 + vectors[1:2]), vectors[0:1]
         ctx_factor, ctx_shift = gain * (1.0 + vectors[4:5]), vectors[3:4]
@@ -421,24 +447,21 @@
     pairs = rows_dev // 2
     chips = n_tp // 2
 
-    turned = offset_bias[:, :, ::-1]
-    early = jnp.pad(turned, ((0, 0), (0, 1), (0, 0)))
-    later = jnp.pad(turned, ((0, 0), (1, 0), (0, 0)))
-    reach = WIN_W - 1
-    gap = jnp.zeros((heads, TABLE, GRID_W - 2 * reach - 1), F32)
-    lines = jnp.concatenate(
-        [early[..., reach:], gap, later, gap, early[..., :reach]], axis=-1
-    )
-
     vmem = pl.BlockSpec(memory_space=pltpu.VMEM)
-    anywhere = pl.BlockSpec(memory_space=pl.ANY)
+    anywhere = pl.BlockSpec(memory_space=pltpu.HBM)
     dma = pltpu.SemaphoreType.DMA
     return pl.pallas_call(
         functools.partial(kernel, n_sp, n_tp),
         out_shape=jax.ShapeDtypeStruct((tokens, cols), BF16),
-        in_specs=[vmem] * 5 + [anywhere] * 8,
+        in_specs=[anywhere] * 13,
         out_specs=vmem,
         scratch_shapes=[
+            pltpu.VMEM(conditioning.shape, BF16),
+            pltpu.VMEM(ctx_vector.shape, BF16),
+            pltpu.VMEM(norm_gain.shape, BF16),
+            pltpu.VMEM(context.shape, BF16),
+            pltpu.VMEM((TABLE - 1, heads, 2 * WIN_W - 1), F32),
+            pltpu.VMEM((heads, TABLE, PAIR), F32),
             pltpu.VMEM((tokens, width), BF16),
             pltpu.VMEM((3,) + w_shift.shape, BF16),
             pltpu.VMEM((3,) + w_query.shape, BF16),
@@ -451,7 +474,7 @@
             pltpu.VMEM((key_rows, 2 * head_width), BF16),
             pltpu.VMEM((heads // 2, TABLE, GRID_W, 2 * PAIR), F32),
             pltpu.VMEM((n_tp, tokens, head_width), BF16),
-            dma((8,)),
+            dma((13,)),
             dma((n_sp,)),
             dma((n_sp,)),
             dma((n_tp,)),
@@ -464,14 +487,14 @@
             dma((pairs, n_tp)),
         ],
         compiler_params=pltpu.CompilerParams(
-            collective_id=0, has_side_effects=True, vmem_limit_bytes=48 * 1024 * 1024
+            collective_id=0, has_side_effects=True, vmem_limit_bytes=67_043_328
         ),
     )(
-        conditioning.reshape(1, -1),
-        ctx_vector.reshape(1, -1),
-        norm_gain.reshape(1, -1),
+        conditioning,
+        ctx_vector,
+        norm_gain,
         context,
-        lines,
+        offset_bias.transpose(1, 0, 2),
         latent,
         w_shift,
         w_scale,

time: 43.8 us -> 34.6 us (0.79)
  the two profiles are of different devices: /device:TPU:9 before, /device:TPU:0 now
where the time goes in v2:
time: 34.6 us; the launch traced here: 33.9 us
  Pallas kernels  32.2 us (93%)
  local copies, waits for them, and re-layouts  1.77 us (5%)
    pallas_call x1, Pallas kernels, local(): pl.pallas_call(functools.partial(kernel, n_sp, n_tp), out_shape=jax.Shape...  32.2 us
    unnamed x1, local copies, waits for them, and re-layouts  1.77 us

profile of v2, /device:TPU:0, one launch (start us, length us, event | category | flops | bytes accessed | tf_op | source)
XLA Modules:
  0.0 33.9 jit_solution(4762890693769173801)
XLA Ops:
  0.0 32.2 %shard_map.127 = bf16[384,512]{1,0:T(8,128)(2,1)} custom-call(bf16[512]{0:T(512)(128)(2,1)} %cond_hbm.1, bf16[512]{0:T(512)(128)(2,1)} %ctxv_hbm.1, bf16[2048]{0:T(1024)(128)(2,1)} %gain_hbm.1, bf16[16,2048]{1,0:T(8,128)(2,1)} %context_hbm.1, f32[15,4,31]{2,1,0:T(4,128)} %bitcast.1, bf16[384,2048]{1,0:T(8,128)(2,1)} %lat_hbm.1, bf16[512,512]{1,0:T(8,128)(2,1)} %wsh_hbm.1, ...), custom_call_target="tpu_custom_call" | custom-call | tf_op jit(solution)/shard_map/pallas_call | solution.py:453
  32.2 1.8 %copy.15 = bf16[384,512]{1,0:T(8,128)(2,1)} copy(bf16[384,512]{1,0:T(8,128)(2,1)} %shard_map.127) | data formatting | bytes 786432

commit v3 on v2

--- a/solution.py
+++ b/solution.py
@@ -162,6 +162,113 @@
     block = context_ref[...].astype(F32)
     inv_ctx = lax.rsqrt(jnp.mean(block * block, axis=-1, keepdims=True) + EPSILON)
 
+    @pl.when(sp == 0)
+    def _():
+        kv[0:own0, :] = jnp.zeros((own0, 2 * head_width), BF16)
+
+    @pl.when(sp == n_sp - 1)
+    def _():
+        kv[high0:ctx0, :] = jnp.zeros((ctx0 - high0, 2 * head_width), BF16)
+
+    for peer in sp_peers:
+        part_copy(peer, peer).wait_recv()
+    summed = part[0]
+    for k in range(1, n_sp):
+        summed = summed + part[k]
+    mod[tp] = summed
+
+    def mod_copy(slot, peer):
+        return pltpu.make_async_remote_copy(
+            src_ref=mod.at[slot],
+            dst_ref=mod.at[slot],
+            send_sem=mod_send.at[peer],
+            recv_sem=mod_recv.at[slot],
+            device_id={"tp": peer},
+            device_id_type=MESH,
+        )
+
+    mod_sends = [mod_copy(tp, peer) for peer in tp_peers]
+    for copy in mod_sends:
+        copy.start()
+    for copy in part_sends:
+        copy.wait_send()
+    for peer in tp_peers:
+        mod_copy(peer, peer).wait_recv()
+
+    for t in range(n_tp):
+        span = slice(t * cols, (t + 1) * cols)
+        gain = gain_ref[span].astype(F32).reshape(1, -1)
+        vectors = mod[t]
+        factor, shift = gain * (1.0 + vectors[1:2]), vectors[0:1]
+        ctx_factor, ctx_shift = gain * (1.0 + vectors[4:5]), vectors[3:4]
+        for r in range(rows_dev):
+            rows = slice(r * GRID_W, (r + 1) * GRID_W)
+            normed[rows, span] = (
+                lat[rows, span].astype(F32) * inv_ref[rows, 0:1] * factor + shift
+            ).astype(BF16)
+        normed[tokens:, span] = (
+            context_ref[:, span].astype(F32) * inv_ctx * ctx_factor + ctx_shift
+        ).astype(BF16)
+
+    def halo_up(i):
+        lanes = pl.ds(i * head_width, head_width)
+        return pltpu.make_async_remote_copy(
+            src_ref=kv.at[pl.ds(high0 - own0, own0), lanes],
+            dst_ref=kv.at[pl.ds(0, own0), lanes],
+            send_sem=halo_send.at[i],
+            recv_sem=halo_recv.at[i],
+            device_id={"sp": lax.rem(sp + 1, n_sp)},
+            device_id_type=MESH,
+        )
+
+    def halo_down(i):
+        lanes = pl.ds(i * head_width, head_width)
+        return pltpu.make_async_remote_copy(
+            src_ref=kv.at[pl.ds(own0, HIGH * GRID_W), lanes],
+            dst_ref=kv.at[pl.ds(high0, HIGH * GRID_W), lanes],
+            send_sem=halo_send.at[2 + i],
+            recv_sem=halo_recv.at[2 + i],
+            device_id={"sp": lax.rem(sp + n_sp - 1, n_sp)},
+            device_id_type=MESH,
+        )
+
+    ups, downs = [halo_up(0), halo_up(1)], [halo_down(0), halo_down(1)]
+    ctx_own_rows = pl.ds(pl.multiple_of(ctx0 + sp * ctx_own, ctx_own), ctx_own)
+    for i in range(2):
+        loads[4 + i].wait()
+        product = jnp.dot(normed[...], wqkv[1 + i], preferred_element_type=F32).astype(BF16)
+        lanes = slice(i * head_width, (i + 1) * head_width)
+        kv[own0:high0, lanes] = product[:tokens]
+        kv[ctx_own_rows, lanes] = product[tokens:]
+
+        @pl.when(sp < n_sp - 1)
+        def _(i=i):
+            ups[i].start()
+
+        @pl.when(sp > 0)
+        def _(i=i):
+            downs[i].start()
+
+    def ctx_copy(slot, peer):
+        rows = pl.ds(pl.multiple_of(ctx0 + slot * ctx_own, ctx_own), ctx_own)
+        return pltpu.make_async_remote_copy(
+            src_ref=kv.at[rows],
+            dst_ref=kv.at[rows],
+            send_sem=ctx_send.at[peer],
+            recv_sem=ctx_recv.at[slot],
+            device_id={"sp": peer},
+            device_id_type=MESH,
+        )
+
+    ctx_sends = [ctx_copy(sp, peer) for peer in sp_peers]
+    for copy in ctx_sends:
+        copy.start()
+
+    loads[6].wait()
+    qbuf[...] = (
+        jnp.dot(normed[:tokens], wqkv[0], preferred_element_type=F32) * HEAD_DIM ** (-0.5)
+    ).astype(BF16)
+
     key_col = lax.broadcasted_iota(jnp.int32, (GRID_W, PAIR), 0)
     lane = lax.broadcasted_iota(jnp.int32, (GRID_W, PAIR), 1)
     query_col = jnp.where(lane >= GRID_W, lane - GRID_W, lane)
@@ -191,119 +298,20 @@
 
             lax.fori_loop(0, TABLE, expand, 0)
 
-    @pl.when(sp == 0)
-    def _():
-        kv[0:own0, :] = jnp.zeros((own0, 2 * head_width), BF16)
-
-    @pl.when(sp == n_sp - 1)
-    def _():
-        kv[high0:ctx0, :] = jnp.zeros((ctx0 - high0, 2 * head_width), BF16)
-
-    for peer in sp_peers:
-        part_copy(peer, peer).wait_recv()
-    summed = part[0]
-    for k in range(1, n_sp):
-        summed = summed + part[k]
-    mod[tp] = summed
-
-    def mod_copy(slot, peer):
-        return pltpu.make_async_remote_copy(
-            src_ref=mod.at[slot],
-            dst_ref=mod.at[slot],
-            send_sem=mod_send.at[peer],
-            recv_sem=mod_recv.at[slot],
-            device_id={"tp": peer},
-            device_id_type=MESH,
-        )
-
-    mod_sends = [mod_copy(tp, peer) for peer in tp_peers]
-    for copy in mod_sends:
-        copy.start()
-    for copy in part_sends:
-        copy.wait_send()
-    for peer in tp_peers:
-        mod_copy(peer, peer).wait_recv()
-
-    for t in range(n_tp):
-        span = slice(t * cols, (t + 1) * cols)
-        gain = gain_ref[span].astype(F32).reshape(1, -1)
-        vectors = mod[t]
-        factor, shift = gain * (1.0 + vectors[1:2]), vectors[0:1]
-        ctx_factor, ctx_shift = gain * (1.0 + vectors[4:5]), vectors[3:4]
-        for r in range(rows_dev):
-            rows = slice(r * GRID_W, (r + 1) * GRID_W)
-            normed[rows, span] = (
-                lat[rows, span].astype(F32) * inv_ref[rows, 0:1] * factor + shift
-            ).astype(BF16)
-        normed[tokens:, span] = (
-            context_ref[:, span].astype(F32) * inv_ctx * ctx_factor + ctx_shift
-        ).astype(BF16)
-
-    ctx_own_rows = pl.ds(pl.multiple_of(ctx0 + sp * ctx_own, ctx_own), ctx_own)
-    for i in range(2):
-        loads[4 + i].wait()
-        product = jnp.dot(normed[...], wqkv[1 + i], preferred_element_type=F32).astype(BF16)
-        lanes = slice(i * head_width, (i + 1) * head_width)
-        kv[own0:high0, lanes] = product[:tokens]
-        kv[ctx_own_rows, lanes] = product[tokens:]
-
-    up = pltpu.make_async_remote_copy(
-        src_ref=kv.at[pl.ds(high0 - own0, own0)],
-        dst_ref=kv.at[pl.ds(0, own0)],
-        send_sem=halo_send.at[0],
-        recv_sem=halo_recv.at[0],
-        device_id={"sp": lax.rem(sp + 1, n_sp)},
-        device_id_type=MESH,
-    )
-    down = pltpu.make_async_remote_copy(
-        src_ref=kv.at[pl.ds(own0, HIGH * GRID_W)],
-        dst_ref=kv.at[pl.ds(high0, HIGH * GRID_W)],
-        send_sem=halo_send.at[1],
-        recv_sem=halo_recv.at[1],
-        device_id={"sp": lax.rem(sp + n_sp - 1, n_sp)},
-        device_id_type=MESH,
-    )
-
-    def ctx_copy(slot, peer):
-        rows = pl.ds(pl.multiple_of(ctx0 + slot * ctx_own, ctx_own), ctx_own)
-        return pltpu.make_async_remote_copy(
-            src_ref=kv.at[rows],
-            dst_ref=kv.at[rows],
-            send_sem=ctx_send.at[peer],
-            recv_sem=ctx_recv.at[slot],
-            device_id={"sp": peer},
-            device_id_type=MESH,
-        )
-
-    ctx_sends = [ctx_copy(sp, peer) for peer in sp_peers]
-    for copy in ctx_sends:
-        copy.start()
-
-    @pl.when(sp < n_sp - 1)
-    def _():
-        up.start()
-
-    @pl.when(sp > 0)
-    def _():
-        down.start()
-
-    loads[6].wait()
-    qbuf[...] = (
-        jnp.dot(normed[:tokens], wqkv[0], preferred_element_type=F32) * HEAD_DIM ** (-0.5)
-    ).astype(BF16)
-
     for copy in mod_sends:
         copy.wait_send()
     for peer in sp_peers:
         ctx_copy(peer, peer).wait_recv()
 
-    @pl.when(sp > 0)
-    def _():
-        up.wait_recv()
-
     @pl.when(sp < n_sp - 1)
     def _():
-        down.wait_recv()
+        for copy in downs:
+            copy.wait_recv()
+
+    @pl.when((sp > 0) & (sp == n_sp - 1))
+    def _():
+        for copy in ups:
+            copy.wait_recv()
 
     partner = tp + 1 - 2 * lax.rem(tp, 2)
     chips = n_tp // 2
@@ -330,7 +338,15 @@
         return jnp.clip(row_base + i - WIN_H // 2, 0, grid_rows - WIN_H) - row_base + LOW
 
     att_sends = []
-    for b in range(pairs):
+    order = list(range(pairs))[::-1]
+    for turn, b in enumerate(order):
+        if turn == 1:
+
+            @pl.when((sp > 0) & (sp < n_sp - 1))
+            def _():
+                for copy in ups:
+                    copy.wait_recv()
+
         i = 2 * b
         start = start_of(i)
         moved = start_of(i + 1) - start
@@ -382,17 +398,21 @@
             copy.start()
         att_sends += sends
 
-    for b in range(pairs):
-        for k, peer in enumerate(others):
-            att_copy(b, peer, peer, 1 + k).wait_recv()
-            forward = att_copy(b, peer, partner, chips + k)
-            forward.start()
-            att_sends.append(forward)
-
     loads[7].wait()
     gate = mod[tp][2:3]
     own_cols = pl.ds(pl.multiple_of(tp * cols, cols), cols)
-    for b in range(pairs):
+
+    def forward(b):
+        for k, peer in enumerate(others):
+            att_copy(b, peer, peer, 1 + k).wait_recv()
+            copy = att_copy(b, peer, partner, chips + k)
+            copy.start()
+            att_sends.append(copy)
+
+    forward(order[0])
+    for turn, b in enumerate(order):
+        if turn + 1 < pairs:
+            forward(order[turn + 1])
         rows = slice(b * PAIR, (b + 1) * PAIR)
         att_copy(b, partner, partner, 0).wait_recv()
         for k, peer in enumerate(others):
@@ -413,11 +433,13 @@
 
     @pl.when(sp < n_sp - 1)
     def _():
-        up.wait_send()
+        for copy in ups:
+            copy.wait_send()
 
     @pl.when(sp > 0)
     def _():
-        down.wait_send()
+        for copy in downs:
+            copy.wait_send()
 
 
 def local(
@@ -481,8 +503,8 @@
             dma((n_tp,)),
             dma((n_sp,)),
             dma((n_sp,)),
-            dma((2,)),
-            dma((2,)),
+            dma((4,)),
+            dma((4,)),
             dma((pairs, 2 * chips)),
             dma((pairs, n_tp)),
         ],

time: 34.6 us -> 32.6 us (0.942)
  Pallas kernels: 32.2 us -> 30.4 us
    pallas_call x1, Pallas kernels: 32.2 us -> 30.4 us  [local(): pl.pallas_call(functools.partial(kernel, n_sp, n_tp), out_shape=jax.Shape...]
where the time goes in v3:
time: 32.6 us; the launch traced here: 32.2 us
  Pallas kernels  30.4 us (93%)
  local copies, waits for them, and re-layouts  1.77 us (5%)
    pallas_call x1, Pallas kernels, local(): pl.pallas_call(functools.partial(kernel, n_sp, n_tp), out_shape=jax.Shape...  30.4 us
    unnamed x1, local copies, waits for them, and re-layouts  1.77 us

profile of v3, /device:TPU:0, one launch (start us, length us, event | category | flops | bytes accessed | tf_op | source)
XLA Modules:
  0.0 32.2 jit_solution(14282887114166330822)
XLA Ops:
  0.0 30.4 %shard_map.127 = bf16[384,512]{1,0:T(8,128)(2,1)} custom-call(bf16[512]{0:T(512)(128)(2,1)} %cond_hbm.1, bf16[512]{0:T(512)(128)(2,1)} %ctxv_hbm.1, bf16[2048]{0:T(1024)(128)(2,1)} %gain_hbm.1, bf16[16,2048]{1,0:T(8,128)(2,1)} %context_hbm.1, f32[15,4,31]{2,1,0:T(4,128)} %bitcast.1, bf16[384,2048]{1,0:T(8,128)(2,1)} %lat_hbm.1, bf16[512,512]{1,0:T(8,128)(2,1)} %wsh_hbm.1, ...), custom_call_target="tpu_custom_call" | custom-call | tf_op jit(solution)/shard_map/pallas_call | solution.py:475
  30.4 1.8 %copy.15 = bf16[384,512]{1,0:T(8,128)(2,1)} copy(bf16[384,512]{1,0:T(8,128)(2,1)} %shard_map.127) | data formatting | bytes 786432
